TPU v7x, 32 devices: a whole 2x2x4 slice. The times are simulated.
32 devices in a mesh: ep: 8 (over z, core), tp: 4 (over y, x).
Axes of the slice: x: 2, y: 2, z: 4, core: 2. Of those that a mesh axis runs over, the one named last changes fastest.
Arguments:
- recurrence_queries: bfloat16 [4096, 2048], P('ep', 'tp'), may hold values from -6 to 6
- forget_preact: bfloat16 [4096, 2048], P('ep', 'tp')
- recurrence_values: bfloat16 [4096, 2048], P('ep', 'tp'), may hold values from -6 to 6
- output_gate_preact: bfloat16 [4096, 2048], P('ep', 'tp'), may hold values from -6 to 6
- forget_floor_logits: float32 [2048], P('tp')
- surge_log_decay: float32 [4096, 16], P('ep', 'tp'), may hold values from -0.7 to 0
- head_norm_gain: float32 [128], replicated, may hold values from 0.1 to 1.9
- recurrence_out_weight: bfloat16 [2048, 2048], P(None, 'tp'), may hold values from -0.125 to 0.125
- second_micro_rows: bfloat16 [1024, 2048], P('ep'), may hold values from -6 to 6
- expert_norm_gain: float32 [2048], replicated, may hold values from 0.1 to 1.9
- row_group_index: int32 [1024], P('ep'), may hold values from 0 to 3, as said below
- group_expert_index: int32 [1024, 2], P('ep'), may hold values from 0 to 7, as said below
- chosen_expert_weight: float32 [1024, 2], P('ep'), may hold values from 0.2 to 1
- expert_gate_weight: bfloat16 [32, 2048, 4096], P('ep', None, 'tp'), may hold values from -0.125 to 0.125
- expert_up_weight: bfloat16 [32, 2048, 4096], P('ep', None, 'tp'), may hold values from -0.125 to 0.125
- expert_down_weight: bfloat16 [32, 4096, 2048], P('ep', None, 'tp'), may hold values from -0.09375 to 0.09375
Outputs:
- mixed: bfloat16 [4096, 2048], P('ep', 'tp')
- expert_out: bfloat16 [1024, 2048], P('ep', 'tp')
Inputs may be any that keep to these rules, and one draw needn't show every extreme that they name: group_expert_index names two different experts of the row's group; the expert's number is row_group_index * 8 + group_expert_index. Among the rows of one index of ep no expert is named more than 12 times, and some expert exactly 12 times. `group_expert_index`: the two entries of a row differ.
All inputs are finite; a program needn't handle non-finite values.
Results may differ from a plain program's by a relative error of at most 0.009.
Values may be sent and summed in bfloat16 or wider, within the bound.
A program may use at most 128 MiB of HBM per device.

v0:
```python
import functools

import jax
import jax.numpy as jnp
import numpy as np
from jax import lax
from jax.experimental import pallas as pl
from jax.experimental.pallas import tpu as pltpu
from jax.sharding import PartitionSpec as P

SPAN = 128
GROUPS = 4
CAP = 12
NORM_EPS = 1e-06
TAIL = 16
MESH = pl.DeviceIdType.MESH

NT = (((1,), (1,)), ((), ()))
TN = (((0,), (0,)), ((), ()))


def span_levels(span):
    return span.bit_length() - 1


def log_sum_matrix(span):
    row, col = np.arange(span)[:, None], np.arange(span)[None, :]
    parts = [col <= row, col > row]
    for level in range(span_levels(span)):
        half = 1 << level
        mid = row // (2 * half) * (2 * half) + half - 1
        later = (row & half) != 0
        parts.append(np.where(later, (col > mid) & (col <= row), (col > row) & (col <= mid)))
    stack = np.stack(parts).astype(np.float32)
    return np.concatenate([stack, stack], axis=2)


def high_low(value):
    high = value.astype(jnp.bfloat16)
    return high, (value - high.astype(jnp.float32)).astype(jnp.bfloat16)


def dot(a, b, dims=(((1,), (0,)), ((), ()))):
    return lax.dot_general(a, b, dims, preferred_element_type=jnp.float32)


def recurrence_kernel(heads, q_ref, f_ref, v_ref, floor_ref, surge_ref, sums_ref,
                      out_ref, decayed_ref, ending_ref, state, carry):
    span, width = q_ref.shape
    key, val = width // heads, v_ref.shape[1] // heads

    @pl.when(pl.program_id(0) == 0)
    def _():
        state[...] = jnp.zeros_like(state)
        carry[...] = jnp.zeros_like(carry)

    rate = jax.nn.sigmoid(-floor_ref[...])
    gate = rate * jax.nn.sigmoid(-f_ref[...].astype(jnp.float32))
    surge = surge_ref[...]
    surge = jnp.concatenate(
        [jnp.broadcast_to(surge[:, h:h + 1], (span, key)) for h in range(heads)], axis=1
    )
    forget = jnp.log1p(-gate) + surge
    query = jax.nn.silu(q_ref[...].astype(jnp.float32))
    pieces = jnp.concatenate(high_low(forget), axis=0)

    row = lax.broadcasted_iota(jnp.int32, (span, span), 0)
    col = lax.broadcasted_iota(jnp.int32, (span, span), 1)
    wide_row = lax.broadcasted_iota(jnp.int32, (span, width), 0)

    own = query * gate
    scores = []
    for h in range(heads):
        same = jnp.sum(own[:, h * key:(h + 1) * key], axis=1, keepdims=True)
        scores.append(jnp.where(row == col, same, 0.0))
    for level in range(span_levels(span)):
        half = 1 << level
        decay = jnp.exp(dot(sums_ref[2 + level], pieces))
        side = (jnp.where((wide_row & half) != 0, query, gate) * decay).astype(jnp.bfloat16)
        met = (((row ^ col) >> level) == 1) & ((row & half) != 0)
        for h in range(heads):
            part = side[:, h * key:(h + 1) * key]
            scores[h] = jnp.where(met, dot(part, part, NT), scores[h])

    since = dot(sums_ref[0], pieces)
    until = dot(sums_ref[1], pieces)
    total = since[span - 1:span, :]
    entered = query * jnp.exp(since)
    leaving = (gate * jnp.exp(until)).astype(jnp.bfloat16)
    decayed_ref[...] = (entered * jnp.exp(carry[...])).astype(jnp.bfloat16)
    entered = entered.astype(jnp.bfloat16)
    kept = jnp.exp(total)
    for h in range(heads):
        keys, vals = slice(h * key, (h + 1) * key), slice(h * val, (h + 1) * val)
        values = v_ref[:, vals]
        held = state[h]
        out_ref[:, vals] = dot(scores[h].astype(jnp.bfloat16), values) + dot(
            entered[:, keys], held.astype(jnp.bfloat16), NT
        )
        state[h] = kept[:, keys] * held + dot(values, leaving[:, keys], TN)
    carry[...] = carry[...] + total

    @pl.when(pl.program_id(0) == pl.num_programs(0) - 1)
    def _():
        high, low = high_low(carry[...])
        for h in range(heads):
            keys = slice(h * key, (h + 1) * key)
            ending_ref[h, :val, :] = state[h].astype(jnp.bfloat16)
            ending_ref[h, val:, :] = jnp.concatenate(
                [high[:, keys], low[:, keys], jnp.zeros((TAIL - 2, key), jnp.bfloat16)], axis=0
            )


def finish_kernel(heads, part_ref, decayed_ref, gate_ref, gain_ref, ends_ref, out_ref, state):
    count = ends_ref.shape[0]
    key = decayed_ref.shape[1] // heads
    val = part_ref.shape[1] // heads
    mine = lax.axis_index("ep")

    @pl.when(pl.program_id(0) == 0)
    def _():
        for h in range(heads):
            def hop(place, held, h=h):
                ending = ends_ref[place, h].astype(jnp.float32)
                kept = jnp.exp(ending[val:val + 1] + ending[val + 1:val + 2])
                return jnp.where(place < mine, kept * held + ending[:val], held)

            held = lax.fori_loop(0, count - 1, hop, jnp.zeros((val, key), jnp.float32))
            state[h] = held.astype(jnp.bfloat16)

    gain = gain_ref[...]
    for h in range(heads):
        keys, vals = slice(h * key, (h + 1) * key), slice(h * val, (h + 1) * val)
        out = part_ref[:, vals] + dot(decayed_ref[:, keys], state[h], NT)
        scale = lax.rsqrt(jnp.mean(out * out, axis=-1, keepdims=True) + NORM_EPS)
        gated = out * scale * gain * jax.nn.silu(gate_ref[:, vals].astype(jnp.float32))
        out_ref[:, vals] = gated.astype(jnp.bfloat16)


def mixer_part(queries, forget, values, floor, surge):
    rows, width = queries.shape
    heads = surge.shape[1]
    key, val = width // heads, values.shape[1] // heads
    span = SPAN
    sums = jnp.asarray(log_sum_matrix(span), jnp.bfloat16)
    tile = lambda w: pl.BlockSpec((span, w), lambda i: (i, 0))
    full = lambda *s: pl.BlockSpec(s, lambda i: (0,) * len(s))
    return pl.pallas_call(
        functools.partial(recurrence_kernel, heads),
        grid=(rows // span,),
        in_specs=[tile(width), tile(width), tile(values.shape[1]), full(1, width), tile(heads),
                  full(*sums.shape)],
        out_specs=[tile(values.shape[1]), tile(width), full(heads, val + TAIL, key)],
        out_shape=[
            jax.ShapeDtypeStruct((rows, values.shape[1]), jnp.float32),
            jax.ShapeDtypeStruct((rows, width), jnp.bfloat16),
            jax.ShapeDtypeStruct((heads, val + TAIL, key), jnp.bfloat16),
        ],
        scratch_shapes=[pltpu.VMEM((heads, val, key), jnp.float32), pltpu.VMEM((1, width), jnp.float32)],
        cost_estimate=pl.CostEstimate(flops=12 * 10**9, bytes_accessed=4 * 10**6, transcendentals=0),
        name="recurrence",
    )(queries, forget, values, floor[None, :], surge, sums)


def mixer_finish(part, decayed, gate, gain, ends):
    rows, width = part.shape
    heads = ends.shape[1]
    val, key = ends.shape[2] - TAIL, ends.shape[3]
    span = SPAN
    tile = lambda w: pl.BlockSpec((span, w), lambda i: (i, 0))
    full = lambda *s: pl.BlockSpec(s, lambda i: (0,) * len(s))
    return pl.pallas_call(
        functools.partial(finish_kernel, heads),
        grid=(rows // span,),
        in_specs=[tile(width), tile(decayed.shape[1]), tile(width), full(1, val), full(*ends.shape)],
        out_specs=tile(width),
        out_shape=jax.ShapeDtypeStruct((rows, width), jnp.bfloat16),
        scratch_shapes=[pltpu.VMEM((heads, val, key), jnp.bfloat16)],
        cost_estimate=pl.CostEstimate(flops=4 * 10**9, bytes_accessed=4 * 10**6, transcendentals=0),
        name="finish",
    )(part, decayed, gate, gain[None, :], ends)


def expert_kernel(x_ref, gate_ref, up_ref, down_ref, out_ref, rows, hidden, gate_buf, up_buf, down_buf,
                  gate_sem, up_sem, down_sem, row_out, row_in, hid_out, hid_in):
    experts, count, _, depth = rows.shape
    part = hidden.shape[3]
    tile, down_tile = gate_buf.shape[2], down_buf.shape[2]
    tiles, down_tiles = gate_buf.shape[0], down_buf.shape[0]
    me = lax.axis_index("tp")

    def hidden_loads(e, j):
        columns = pl.ds(j * tile, tile)
        return (
            pltpu.make_async_copy(gate_ref.at[e, :, columns], gate_buf.at[j], gate_sem.at[j]),
            pltpu.make_async_copy(up_ref.at[e, :, columns], up_buf.at[j], up_sem.at[j]),
        )

    def down_load(e, j):
        columns = pl.ds(j * down_tile, down_tile)
        return pltpu.make_async_copy(down_ref.at[e, :, columns], down_buf.at[j], down_sem.at[j])

    def peer(d):
        return lax.rem(me + d, count)

    def row_copy(e, d):
        return pltpu.make_async_remote_copy(
            src_ref=x_ref.at[e], dst_ref=rows.at[e, me], send_sem=row_out.at[e, d - 1],
            recv_sem=row_in.at[e, d - 1], device_id={"tp": peer(d)}, device_id_type=MESH,
        )

    def hidden_copy(e, d):
        return pltpu.make_async_remote_copy(
            src_ref=hidden.at[e, me], dst_ref=hidden.at[e, me], send_sem=hid_out.at[e, d - 1],
            recv_sem=hid_in.at[e, d - 1], device_id={"tp": peer(d)}, device_id_type=MESH,
        )

    barrier = pltpu.get_barrier_semaphore()
    for d in range(1, count):
        pl.semaphore_signal(barrier, inc=1, device_id={"tp": peer(d)}, device_id_type=MESH)
    for j in range(tiles):
        for load in hidden_loads(0, j):
            load.start()
    for e in range(experts):
        rows[e, me] = x_ref[e]
    pl.semaphore_wait(barrier, count - 1)
    for e in range(experts):
        for d in range(1, count):
            row_copy(e, d).start()
    for j in range(down_tiles):
        down_load(0, j).start()

    @pl.loop(0, experts)
    def _(e):
        for d in range(1, count):
            row_copy(e, d).wait_recv()
        for j in range(tiles):
            for load in hidden_loads(e, j):
                load.wait()
            gate, up = 0.0, 0.0
            for s in range(count):
                piece = rows[e, s]
                gate += dot(piece, gate_buf[j, s * depth:(s + 1) * depth])
                up += dot(piece, up_buf[j, s * depth:(s + 1) * depth])
            hidden[e, me, :, j * tile:(j + 1) * tile] = (jax.nn.silu(gate) * up).astype(jnp.bfloat16)

            @pl.when(e < experts - 1)
            def _():
                for load in hidden_loads(e + 1, j):
                    load.start()

        for d in range(1, count):
            hidden_copy(e, d).start()

    @pl.loop(0, experts)
    def _(e):
        for d in range(1, count):
            hidden_copy(e, d).wait_recv()
        for j in range(down_tiles):
            down_load(e, j).wait()
            total = 0.0
            for s in range(count):
                total += dot(hidden[e, s], down_buf[j, s * part:(s + 1) * part])
            out_ref[e, :, j * down_tile:(j + 1) * down_tile] = total.astype(jnp.bfloat16)

            @pl.when(e < experts - 1)
            def _():
                down_load(e + 1, j).start()

    @pl.loop(0, experts)
    def _(e):
        for d in range(1, count):
            row_copy(e, d).wait_send()
            hidden_copy(e, d).wait_send()


def expert_layer(arrived, gate, up, down):
    experts, slots, depth = arrived.shape
    count = lax.axis_size("tp")
    part, width = gate.shape[2], down.shape[2]
    tile, down_tile = min(256, part), min(256, width)
    vmem = pl.BlockSpec(memory_space=pltpu.VMEM)
    hbm = pl.BlockSpec(memory_space=pl.ANY)
    dma = pltpu.SemaphoreType.DMA
    size = gate.size + up.size + down.size
    return pl.pallas_call(
        expert_kernel,
        in_specs=[vmem, hbm, hbm, hbm],
        out_specs=vmem,
        out_shape=jax.ShapeDtypeStruct((experts, slots, width), jnp.bfloat16),
        scratch_shapes=[
            pltpu.VMEM((experts, count, slots, depth), jnp.bfloat16),
            pltpu.VMEM((experts, count, slots, part), jnp.bfloat16),
            pltpu.VMEM((part // tile, gate.shape[1], tile), jnp.bfloat16),
            pltpu.VMEM((part // tile, up.shape[1], tile), jnp.bfloat16),
            pltpu.VMEM((width // down_tile, down.shape[1], down_tile), jnp.bfloat16),
            dma((part // tile,)), dma((part // tile,)), dma((width // down_tile,)),
        ] + [dma((experts, count - 1))] * 4,
        compiler_params=pltpu.CompilerParams(
            collective_id=1, has_side_effects=True, vmem_limit_bytes=36 * 2**20
        ),
        cost_estimate=pl.CostEstimate(
            flops=4 * slots * size, bytes_accessed=4 * size, transcendentals=0
        ),
        name="experts",
    )(arrived, gate, up, down)


def token_mixing_layer(
    recurrence_queries,
    forget_preact,
    recurrence_values,
    output_gate_preact,
    forget_floor_logits,
    surge_log_decay,
    head_norm_gain,
):
    part, decayed, ending = mixer_part(
        recurrence_queries, forget_preact, recurrence_values, forget_floor_logits, surge_log_decay
    )
    ends = lax.all_gather(ending, "ep")
    gated_heads = mixer_finish(part, decayed, output_gate_preact, head_norm_gain, ends)
    return gated_heads


def mixer_project(gated_heads, recurrence_out_weight):
    return jnp.dot(
        lax.all_gather(gated_heads, "tp", axis=1, tiled=True),
        recurrence_out_weight,
        preferred_element_type=jnp.float32,
    ).astype(jnp.bfloat16)


def routed_experts(
    gated_heads,
    second_micro_rows,
    expert_norm_gain,
    row_group_index,
    group_expert_index,
    chosen_expert_weight,
    expert_gate_weight,
    expert_up_weight,
    expert_down_weight,
):
    row_count = second_micro_rows.shape[0]
    model_width = second_micro_rows.shape[1]
    columns = model_width // lax.axis_size("tp")
    local_count = expert_gate_weight.shape[0]
    expert_count = local_count * lax.axis_size("ep")
    per_group = expert_count // GROUPS
    rows_float = second_micro_rows.astype(jnp.float32)
    normed_rows = (
        rows_float
        * lax.rsqrt(jnp.mean(rows_float * rows_float, axis=-1, keepdims=True) + NORM_EPS)
        * expert_norm_gain
    ).astype(jnp.bfloat16)
    flat_expert = (row_group_index[:, None] * per_group + group_expert_index).reshape(-1)
    onehot = (flat_expert[:, None] == jnp.arange(expert_count, dtype=jnp.int32)[None, :]).astype(
        jnp.int32
    )
    rank_index = jnp.sum((jnp.cumsum(onehot, axis=0) - onehot) * onehot, axis=1)
    slot_index = flat_expert * CAP + rank_index
    owner_row = (
        jnp.full((expert_count * CAP,), row_count, jnp.int32)
        .at[slot_index]
        .set(jnp.arange(2 * row_count) // 2)
    )
    col_part = lax.dynamic_slice_in_dim(normed_rows, lax.axis_index("tp") * columns, columns, 1)
    padded = jnp.concatenate([col_part, jnp.zeros((1, columns), jnp.bfloat16)], axis=0)
    outgoing = padded[owner_row].reshape(expert_count, CAP, columns)
    arrived = lax.all_to_all(outgoing, "ep", split_axis=0, concat_axis=1, tiled=True)
    arrived, _ = lax.optimization_barrier((arrived, gated_heads))
    result = expert_layer(arrived, expert_gate_weight, expert_up_weight, expert_down_weight)
    returned = lax.all_to_all(result, "ep", split_axis=1, concat_axis=0, tiled=True)
    picked = returned.reshape(expert_count * CAP, expert_down_weight.shape[2])[slot_index]
    picked = picked.reshape(row_count, 2, expert_down_weight.shape[2]).astype(jnp.float32)
    return jnp.sum(picked * chosen_expert_weight[:, :, None], axis=1).astype(jnp.bfloat16)


def local(
    recurrence_queries,
    forget_preact,
    recurrence_values,
    output_gate_preact,
    forget_floor_logits,
    surge_log_decay,
    head_norm_gain,
    recurrence_out_weight,
    second_micro_rows,
    expert_norm_gain,
    row_group_index,
    group_expert_index,
    chosen_expert_weight,
    expert_gate_weight,
    expert_up_weight,
    expert_down_weight,
):
    gated_heads = token_mixing_layer(
        recurrence_queries,
        forget_preact,
        recurrence_values,
        output_gate_preact,
        forget_floor_logits,
        surge_log_decay,
        head_norm_gain,
    )
    mixed = mixer_project(gated_heads, recurrence_out_weight)
    expert_out = routed_experts(
        gated_heads,
        second_micro_rows,
        expert_norm_gain,
        row_group_index,
        group_expert_index,
        chosen_expert_weight,
        expert_gate_weight,
        expert_up_weight,
        expert_down_weight,
    )
    return (mixed, expert_out)


def solution(mesh):
    return jax.shard_map(
        local,
        mesh=mesh,
        in_specs=(
            P("ep", "tp"),
            P("ep", "tp"),
            P("ep", "tp"),
            P("ep", "tp"),
            P("tp"),
            P("ep", "tp"),
            P(),
            P(None, "tp"),
            P("ep", None),
            P(),
            P("ep"),
            P("ep", None),
            P("ep", None),
            P("ep", None, "tp"),
            P("ep", None, "tp"),
            P("ep", None, "tp"),
        ),
        out_specs=(P("ep", "tp"), P("ep", "tp")),
        check_vma=False,
    )
```

profile of v0, /device:TPU:0, one launch (start us, length us, event | category | flops | bytes accessed | tf_op | source)
XLA Modules:
  0.0 171.1 jit_solution(3397567750903967798)
XLA Ops:
  7.2 0.0 copy-start
  7.2 0.0 all-gather.6.cloned.1.call-start
  7.2 1.7 copy.33.surge_ref
  8.9 0.0 copy-start.2
  8.9 0.0 copy-start.5
  8.9 0.0 copy-start.4
  8.9 12.2 %recurrence.1 = (f32[512,512]{1,0:T(8,128)}, bf16[512,512]{1,0:T(8,128)(2,1)}, bf16[4,144,128]{2,1,0:T(8,128)(2,1)}) custom-call(bf16[512,512]{1,0:T(8,128)(2,1)} %q_ref.1, bf16[512,512]{1,0:T(8,128)(2,1)} %f_ref.1, bf16[512,512]{1,0:T(8,128)(2,1)} %v_ref.1, f32[1,512]{1,0:T(1,128)} %bitcast.41, f32[512,4]{1,0:T(8,128)} %copy.33.surge_ref, ...), custom_call_target="tpu_custom_call" | custom-call | flops 12000000000 | bytes 4000000 | tf_op jit(solution)/shard_map/recurrence/pallas_call | solution.py:148
  21.1 0.0 all-gather.6.cloned.1.call-update
  21.2 0.0 all-gather.4.cloned.1.call-start
  21.2 0.0 copy-done.2
  21.2 1.1 convert_element_type.26
  22.3 0.0 copy-done.5
  22.3 0.0 copy-done.4
  22.3 0.1 copy.35
  22.5 0.1 eq.29
  22.6 0.6 reduce-window.6
  23.2 0.8 dynamic-slice
  24.0 0.2 slice_reduce_fusion
  24.1 0.2 multiply_reduce_fusion
  24.3 1.1 fusion.1
  25.4 21.4 %all-gather.6.cloned.1.call-done = bf16[32,144,128]{2,1,0:T(8,128)(2,1)} async-done(((bf16[4,144,128]{2,1,0:T(8,128)(2,1)}), bf16[32,144,128]{2,1,0:T(8,128)(2,1)}) %all-gather.6.cloned.1.call-update) | async-done | bytes 1179664 | tf_op jit(solution)/shard_map/all_gather | solution.py:321
  46.8 5.1 %finish.1 = bf16[512,512]{1,0:T(8,128)(2,1)} custom-call(f32[512,512]{1,0:T(8,128)} %get-tuple-element.6.part_ref, bf16[512,512]{1,0:T(8,128)(2,1)} %get-tuple-element.7.decayed_ref, bf16[512,512]{1,0:T(8,128)(2,1)} %gate_ref.2, f32[1,128]{1,0:T(1,128)} %bitcast.42, bf16[8,4,144,128]{3,2,1,0:T(8,128)(2,1)} %bitcast.40), custom_call_target="tpu_custom_call" | custom-call | flops 4000000000 | bytes 4000000 | tf_op jit(solution)/shard_map/finish/pallas_call | solution.py:172
  52.0 0.0 all-gather.4.cloned.1.call-update
  52.0 0.1 eq.25
  52.1 0.1 copy.34
  52.3 0.1 mul.66
  52.5 0.1 fusion.4
  52.6 1.4 scatter_custom_fusion
  54.0 2.1 %gather_fusion = bf16[384,512]{1,0:T(8,128)(2,1)S(1)} fusion(bf16[129,512]{1,0:T(8,128)(2,1)S(1)} %concatenate.3, s32[1024]{0:T(1024)S(1)} %pad_clamp_fusion.1), kind=kCustom, calls=%fused_computation | custom fusion | bytes 787968 | tf_op jit(solution)/shard_map/gather | solution.py:370
  56.1 0.1 reshape.73
  56.2 18.6 %all_to_all.33 = bf16[32,12,512]{2,1,0:T(8,128)(2,1)S(1)} all-to-all(bf16[32,12,512]{2,1,0:T(8,128)(2,1)S(1)} %reshape.73), channel_id=1, replica_groups=mesh['ep'=8,'tp'=4] {'ep'}, dimensions={0} | all-to-all | bytes 786432 | tf_op jit(solution)/shard_map/all_to_all | solution.py:371
  74.7 0.3 copy.45
  75.0 0.1 copy.40.x_ref
  75.1 0.0 copy-start.1
  75.1 5.8 %copy-done.1 = bf16[4,2048,1024]{2,1,0:T(8,128)(2,1)S(1)} copy-done((bf16[4,2048,1024]{2,1,0:T(8,128)(2,1)S(1)}, bf16[4,2048,1024]{2,1,0:T(8,128)(2,1)}, u32[]{:S(2)}) %copy-start.1) | copy-done | bytes 16777240
  80.9 0.0 copy-start.3
  80.9 58.5 %experts.1 = bf16[4,96,512]{2,1,0:T(8,128)(2,1)S(1)} custom-call(bf16[4,96,512]{2,1,0:T(8,128)(2,1)S(1)} %copy.40.x_ref, bf16[4,2048,1024]{2,1,0:T(8,128)(2,1)S(1)} %copy-done.1, bf16[4,2048,1024]{2,1,0:T(8,128)(2,1)} %up_ref.1, bf16[4,4096,512]{2,1,0:T(8,128)(2,1)} %down_ref.1), custom_call_target="tpu_custom_call" | custom-call | flops 9663676416 | bytes 100663296 | tf_op jit(solution)/shard_map/experts/pallas_call | solution.py:286
  139.4 1.1 copy.41
  140.4 4.6 %all-to-all-start.1 = ((bf16[4,96,512]{2,0,1:T(4,128)(2,1)}), bf16[4,96,512]{2,0,1:T(4,128)(2,1)S(1)}, u32[]{:S(2)}, u32[]{:S(2)}) async-start(bf16[4,96,512]{2,0,1:T(4,128)(2,1)} %copy.41), calls=%async_computation.1 | async-start | bytes 786432 | tf_op jit(solution)/shard_map/all_to_all | solution.py:374
  145.1 0.0 copy-done.3
  145.1 0.1 copy.43
  145.2 12.4 %all-to-all-done.1 = bf16[4,96,512]{2,0,1:T(4,128)(2,1)S(1)} async-done(((bf16[4,96,512]{2,0,1:T(4,128)(2,1)}), bf16[4,96,512]{2,0,1:T(4,128)(2,1)S(1)}, u32[]{:S(2)}, u32[]{:S(2)}) %all-to-all-start.1) | async-done | bytes 393248 | tf_op jit(solution)/shard_map/all_to_all | solution.py:374
  157.6 0.1 copy.42
  157.7 0.1 reshape.74
  157.8 1.2 gather_fusion.1
  158.9 0.3 reshape.75
  159.3 1.4 multiply_reduce_fusion.1
  160.6 0.0 all-gather.4.cloned.1.call-done
  160.6 0.0 copy-done
  160.7 3.6 %convolution_convert_fusion = bf16[512,512]{1,0:T(8,128)(2,1)} fusion(bf16[512,2048]{1,0:T(8,128)(2,1)} %all-gather.4.cloned.1.call-done, bf16[2048,512]{1,0:T(8,128)(2,1)S(1)} %copy-done), kind=kOutput, calls=%fused_computation.3 | convolution fusion | flops 1074003968 | bytes 4718592 | tf_op jit(solution)/shard_map/dot_general | solution.py:327
  (12 shorter events, 0.1 us)
Async XLA Ops:
  7.2 153.5 %copy-start = (bf16[2048,512]{1,0:T(8,128)(2,1)S(1)}, bf16[2048,512]{1,0:T(8,128)(2,1)}, u32[]{:S(2)}) copy-start(bf16[2048,512]{1,0:T(8,128)(2,1)} %param.24) | copy-start | bytes 6291460
  7.2 39.7 %all-gather.6.cloned.1.call-start = ((), (), s32[]{:S(2)}) async-start(), calls=%async_computation.3 | async-start | bytes 1327104 | tf_op jit(solution)/shard_map/all_gather | solution.py:321
  8.9 12.3 %copy-start.2 = (bf16[128,2048]{1,0:T(8,128)(2,1)S(1)}, bf16[128,2048]{1,0:T(8,128)(2,1)}, u32[]{:S(2)}) copy-start(bf16[128,2048]{1,0:T(8,128)(2,1)} %param.25) | copy-start | bytes 1572868
  8.9 13.4 %copy-start.5 = (s32[128]{0:T(128)S(1)}, s32[128]{0:T(128)}, u32[]{:S(2)}) copy-start(s32[128]{0:T(128)} %param.27) | copy-start | bytes 1540
  8.9 13.4 %copy-start.4 = (s32[128,2]{0,1:T(2,128)S(1)}, s32[128,2]{0,1:T(2,128)}, u32[]{:S(2)}) copy-start(s32[128,2]{0,1:T(2,128)} %param.28) | copy-start | bytes 3076
  21.2 139.5 %all-gather.4.cloned.1.call-start = ((), (), s32[]{:S(2)}) async-start(), calls=%async_computation.2 | async-start | bytes 2621440 | tf_op jit(solution)/shard_map/all_gather | solution.py:328
  75.1 5.8 %copy-start.1 = (bf16[4,2048,1024]{2,1,0:T(8,128)(2,1)S(1)}, bf16[4,2048,1024]{2,1,0:T(8,128)(2,1)}, u32[]{:S(2)}) copy-start(bf16[4,2048,1024]{2,1,0:T(8,128)(2,1)} %gate_ref.3) | copy-start | bytes 50331652
  80.9 64.2 %copy-start.3 = (f32[128,2]{0,1:T(2,128)S(1)}, f32[128,2]{0,1:T(2,128)}, u32[]{:S(2)}) copy-start(f32[128,2]{0,1:T(2,128)} %param.29) | copy-start | bytes 3076
  140.4 17.1 %all-to-all-start.1 = ((bf16[4,96,512]{2,0,1:T(4,128)(2,1)}), bf16[4,96,512]{2,0,1:T(4,128)(2,1)S(1)}, u32[]{:S(2)}, u32[]{:S(2)}) async-start(bf16[4,96,512]{2,0,1:T(4,128)(2,1)} %copy.41), calls=%async_computation.1 | async-start | bytes 786432 | tf_op jit(solution)/shard_map/all_to_all | solution.py:374
Sparse Core Ops, SparseCore 0:
  21.3 25.4 all-gather.5
  52.1 39.3 all-gather.3
where the time goes:
time: 172 us; the launch traced here: 171 us
  Pallas kernels  75.8 us (44%)
  waiting for transfers between devices  33.9 us (20%)
  blocking collectives  18.6 us (11%)
  local copies, waits for them, and re-layouts  15.9 us (9%)
  between operations  14.2 us (8%)
  starting transfers between devices  4.69 us (3%)
  other arithmetic  4.47 us (3%)
  matrix products  3.63 us (2%)
    pallas_call x1, Pallas kernels, expert_layer(): pl.pallas_call(expert_kernel, in_specs=[vmem, hbm, hbm, hbm], out_specs=v...  58.5 us
    all_gather x1, waiting for transfers between devices, token_mixing_layer(): ends = lax.all_gather(ending, 'ep')  21.4 us
    all_to_all x1, blocking collectives, routed_experts(): lax.all_to_all(outgoing, 'ep', split_axis=0, concat_axis=1, tiled=True)  18.6 us
    all_to_all x1, waiting for transfers between devices, routed_experts(): lax.all_to_all(result, 'ep', split_axis=1, concat_axis=0, tiled=True)  12.4 us
    pallas_call x1, Pallas kernels, mixer_part(): pl.pallas_call(functools.partial(recurrence_kernel, heads), grid=(rows //...  12.2 us
    unnamed x14, local copies, waits for them, and re-layouts  7.61 us
    pallas_call x1, Pallas kernels, mixer_finish(): pl.pallas_call(functools.partial(finish_kernel, heads), grid=(rows // spa...  5.13 us
    all_to_all x1, starting transfers between devices, routed_experts(): lax.all_to_all(result, 'ep', split_axis=1, concat_axis=0, tiled=True)  4.61 us
  transfers between devices with their start and end apart: 3, of which 2 were waited for; matrix products, arithmetic and copies ran while one was open for 8% of the time, Pallas kernels for 34%

commit v1 on v0

v1 whole, which is shorter than its diff:
```python
import functools

import jax
import jax.numpy as jnp
import numpy as np
from jax import lax
from jax.experimental import pallas as pl
from jax.experimental.pallas import tpu as pltpu
from jax.sharding import PartitionSpec as P

SPAN = 128
GROUPS = 4
CAP = 12
NORM_EPS = 1e-06
TAIL = 16
SOURCE_STEP = 1024
MESH = pl.DeviceIdType.MESH

NN = (((1,), (0,)), ((), ()))
NT = (((1,), (1,)), ((), ()))
TN = (((0,), (0,)), ((), ()))


def span_levels(span):
    return span.bit_length() - 1


def log_sum_matrix(span):
    row, col = np.arange(span)[:, None], np.arange(span)[None, :]
    parts = [col <= row, col > row]
    for level in range(span_levels(span)):
        half = 1 << level
        mid = row // (2 * half) * (2 * half) + half - 1
        later = (row & half) != 0
        parts.append(np.where(later, (col > mid) & (col <= row), (col > row) & (col <= mid)))
    stack = np.stack(parts).astype(np.float32)
    return np.concatenate([stack, stack], axis=2)


def slot_codes(sources, experts, members):
    expert, source, place = np.meshgrid(np.arange(experts), np.arange(sources), np.arange(CAP), indexing="ij")
    code = (source // members * SOURCE_STEP + expert * CAP + place + 1).reshape(-1)
    owner = (source % members).reshape(-1)
    return np.stack([np.where(owner == m, code, -SOURCE_STEP) for m in range(members)], axis=1).astype(np.float32)


def by_source(sources, experts):
    order = np.arange(experts * sources * CAP).reshape(experts, sources, CAP).transpose(1, 0, 2).reshape(-1)
    return np.eye(order.size, dtype=np.float32)[order]


def high_low(value):
    high = value.astype(jnp.bfloat16)
    return high, (value - high.astype(jnp.float32)).astype(jnp.bfloat16)


def dot(a, b, dims=NN):
    return lax.dot_general(a, b, dims, preferred_element_type=jnp.float32)


def aligned(index, step):
    return pl.multiple_of(index * step, step)


class Gather:
    def __init__(self, pick, rows, count, me, send, recv):
        self.pick, self.rows, self.count, self.me, self.send, self.recv = pick, rows, count, me, send, recv
        self.square = count == 4
        self.half = rows // 2

    def copy(self, k, owner, begin, size, peer):
        ref = self.pick(owner, begin, size)
        return pltpu.make_async_remote_copy(
            src_ref=ref, dst_ref=ref, send_sem=self.send(k), recv_sem=self.recv(k),
            device_id={"tp": peer}, device_id_type=MESH,
        )

    def first(self):
        if not self.square:
            return [self.copy(d - 1, self.me, 0, self.rows, lax.rem(self.me + d, self.count))
                    for d in range(1, self.count)]
        return [self.copy(k, self.me, 0, self.rows, self.me ^ (1 << k)) for k in range(2)]

    def second(self):
        if not self.square:
            return []
        return [self.copy(2, self.me ^ 1, 0, self.half, self.me ^ 2),
                self.copy(3, self.me ^ 2, self.half, self.half, self.me ^ 1)]

    def start(self):
        for copy in self.first():
            copy.start()

    def forward(self):
        if self.square:
            for came, passed in zip(self.first(), self.second()):
                came.wait_recv()
                passed.start()

    def finish(self):
        for copy in self.second() if self.square else self.first():
            copy.wait_recv()

    def drain(self):
        for copy in self.first() + self.second():
            copy.wait_send()


def gather_steps(count):
    return 4 if count == 4 else count - 1


def body(
    dims,
    q_hbm, f_hbm, v_hbm, og_hbm, floor_ref, surge_ref, gain_ref, wout_hbm, rows_ref, egain_ref, grp_ref, pick_ref,
    weight_ref, sums_ref, code_ref, order_ref, gate_hbm, up_hbm, down_hbm,
    mixed_ref, expert_ref,
    q_buf, f_buf, v_buf, og_buf, wout_buf, part, decayed, state, carry, ends, heads_all,
    pack, meta_out, meta_in, rows_all, x_buf, hidden, res, ret_out, ret_in, gate_buf, up_buf, down_buf,
    in_sem, gate_sem, up_sem, down_sem,
    z_send, z_recv, m_send, m_recv, t_send, t_recv, d_send, d_recv,
    h_send, h_recv, g_send, g_recv, e_send, e_recv, r_send, r_recv,
):
    n_ep, n_tp, n_groups = dims["ep"], dims["tp"], GROUPS
    members = n_ep // n_groups
    me, mt = lax.axis_index("ep"), lax.axis_index("tp")
    mine_group, mine_member = me // members, lax.rem(me, members)

    length, width = q_buf.shape
    n_heads = surge_ref.shape[0]
    key, val = width // n_heads, v_buf.shape[1] // n_heads
    spans, span = length // SPAN, SPAN
    experts = gate_hbm.shape[0]
    per_group = experts * members
    row_count, model = rows_ref.shape
    quarter = model // n_tp
    room = pack.shape[1]
    lanes = meta_out.shape[2]
    slots = x_buf.shape[1]
    ff = hidden.shape[3]
    tile = min(256, ff)
    out_width = mixed_ref.shape[1]

    def input_load(k):
        pair = [(q_hbm, q_buf), (f_hbm, f_buf), (v_hbm, v_buf), (og_hbm, og_buf), (wout_hbm, wout_buf)][k]
        return pltpu.make_async_copy(pair[0], pair[1], in_sem.at[k])

    def hidden_loads(e, slot):
        return (pltpu.make_async_copy(gate_hbm.at[e], gate_buf.at[slot], gate_sem.at[slot]),
                pltpu.make_async_copy(up_hbm.at[e], up_buf.at[slot], up_sem.at[slot]))

    def down_load(e):
        return pltpu.make_async_copy(down_hbm.at[e], down_buf.at[e], down_sem.at[e])

    barrier = pltpu.get_barrier_semaphore()
    for d in range(1, n_tp):
        pl.semaphore_signal(barrier, inc=1, device_id={"tp": lax.rem(mt + d, n_tp)}, device_id_type=MESH)
    for d in range(1, n_ep):
        pl.semaphore_signal(barrier, inc=1, device_id={"ep": lax.rem(me + d, n_ep)}, device_id_type=MESH)
    for k in range(4):
        input_load(k).start()
    slots_of_weights = gate_buf.shape[0]
    for e in range(min(slots_of_weights, experts)):
        for load in hidden_loads(e, e):
            load.start()
    for e in range(experts):
        down_load(e).start()
    input_load(4).start()

    grp = grp_ref[...]
    picks = [pick_ref[c:c + 1, :] for c in range(2)]
    n_experts = per_group * n_groups
    before = (
        lax.broadcasted_iota(jnp.int32, (row_count, row_count), 0)
        < lax.broadcasted_iota(jnp.int32, (row_count, row_count), 1)
    ).astype(jnp.bfloat16)
    expert_iota = lax.broadcasted_iota(jnp.int32, (n_experts, row_count), 0)
    names = [grp * per_group + pick for pick in picks]
    named = sum((expert_iota == name).astype(jnp.float32) for name in names)
    ranks = dot(named.astype(jnp.bfloat16), before)
    rank = [jnp.sum(jnp.where(expert_iota == name, ranks, 0.0), axis=0, keepdims=True) for name in names]
    group_iota = lax.broadcasted_iota(jnp.int32, (8, row_count), 0)
    in_group = group_iota == grp
    group_ranks = dot(in_group.astype(jnp.bfloat16), before)
    place = jnp.sum(jnp.where(in_group, group_ranks, 0.0), axis=0, keepdims=True).astype(jnp.int32)
    code = [pick * CAP + r.astype(jnp.int32) + 1 for pick, r in zip(picks, rank)]
    column = [name * CAP + r.astype(jnp.int32) for name, r in zip(names, rank)]

    row8 = lax.broadcasted_iota(jnp.int32, (8, row_count), 0)
    codes = jnp.where(row8 == 0, code[0], jnp.where(row8 == 1, code[1], 0)).astype(jnp.float32).astype(jnp.bfloat16)
    for g in range(n_groups):
        spot = lax.broadcasted_iota(jnp.int32, (lanes, row_count), 0)
        at = ((spot == mine_group * room + place) & (grp == g)).astype(jnp.float32).astype(jnp.bfloat16)
        meta_out[g] = dot(codes, at, NT)

    rows_float = rows_ref[...].astype(jnp.float32)
    scale = lax.rsqrt(jnp.mean(rows_float * rows_float, axis=-1, keepdims=True) + NORM_EPS)
    columns = pl.ds(aligned(mt, quarter), quarter)
    normed = (rows_ref[:, columns].astype(jnp.float32) * scale * egain_ref[:, columns]).astype(jnp.bfloat16)
    spot = lax.broadcasted_iota(jnp.int32, (n_groups * room, row_count), 0)
    at = (spot == grp * room + place).astype(jnp.float32).astype(jnp.bfloat16)
    packed = dot(at, normed).astype(jnp.bfloat16)
    for g in range(n_groups):
        pack[g] = packed[g * room:(g + 1) * room]

    def z_copy(d):
        g = lax.rem(mine_group + d, n_groups)
        return pltpu.make_async_remote_copy(
            src_ref=pack.at[g], dst_ref=rows_all.at[mine_member, mt, mine_group], send_sem=z_send.at[d - 1],
            recv_sem=z_recv.at[d - 1], device_id={"ep": g * members + mine_member}, device_id_type=MESH,
        )

    def meta_copy(d):
        to = lax.rem(me + d, n_ep)
        return pltpu.make_async_remote_copy(
            src_ref=meta_out.at[to // members], dst_ref=meta_in.at[me], send_sem=m_send.at[d - 1],
            recv_sem=m_recv.at[d - 1], device_id={"ep": to}, device_id_type=MESH,
        )

    def tp_copy(d):
        ref = rows_all.at[mine_member, mt]
        return pltpu.make_async_remote_copy(
            src_ref=ref, dst_ref=ref, send_sem=t_send.at[d - 1], recv_sem=t_recv.at[d - 1],
            device_id={"tp": lax.rem(mt + d, n_tp)}, device_id_type=MESH,
        )

    def member_copy(d):
        to = mine_group * members + lax.rem(mine_member + d, members)
        ref = rows_all.at[mine_member]
        return pltpu.make_async_remote_copy(
            src_ref=ref, dst_ref=ref, send_sem=d_send.at[d - 1], recv_sem=d_recv.at[d - 1],
            device_id={"ep": to}, device_id_type=MESH,
        )

    pl.semaphore_wait(barrier, n_tp + n_ep - 2)
    for d in range(1, n_groups):
        z_copy(d).start()
    for d in range(1, n_ep):
        meta_copy(d).start()
    rows_all[mine_member, mt, mine_group] = pack[mine_group]
    meta_in[me] = meta_out[mine_group]

    state[...] = jnp.zeros_like(state)
    carry[...] = jnp.zeros_like(carry)
    rate = jax.nn.sigmoid(-floor_ref[...])
    for k in range(3):
        input_load(k).wait()

    @pl.loop(0, spans)
    def _(i):
        at = pl.ds(aligned(i, span), span)
        gate = rate * jax.nn.sigmoid(-f_buf[at, :].astype(jnp.float32))
        surge = jnp.concatenate(
            [jnp.broadcast_to(surge_ref[h:h + 1, at], (key, span)).T for h in range(n_heads)], axis=1
        )
        forget = jnp.log1p(-gate) + surge
        query = jax.nn.silu(q_buf[at, :].astype(jnp.float32))
        pieces = jnp.concatenate(high_low(forget), axis=0)

        row = lax.broadcasted_iota(jnp.int32, (span, span), 0)
        col = lax.broadcasted_iota(jnp.int32, (span, span), 1)
        wide_row = lax.broadcasted_iota(jnp.int32, (span, width), 0)

        own = query * gate
        scores = []
        for h in range(n_heads):
            same = jnp.sum(own[:, h * key:(h + 1) * key], axis=1, keepdims=True)
            scores.append(jnp.where(row == col, same, 0.0))
        for level in range(span_levels(span)):
            half = 1 << level
            decay = jnp.exp(dot(sums_ref[2 + level], pieces))
            side = (jnp.where((wide_row & half) != 0, query, gate) * decay).astype(jnp.bfloat16)
            met = (((row ^ col) >> level) == 1) & ((row & half) != 0)
            for h in range(n_heads):
                piece = side[:, h * key:(h + 1) * key]
                scores[h] = jnp.where(met, dot(piece, piece, NT), scores[h])

        since = dot(sums_ref[0], pieces)
        until = dot(sums_ref[1], pieces)
        total = since[span - 1:span, :]
        entered = query * jnp.exp(since)
        leaving = (gate * jnp.exp(until)).astype(jnp.bfloat16)
        decayed[at, :] = (entered * jnp.exp(carry[...])).astype(jnp.bfloat16)
        entered = entered.astype(jnp.bfloat16)
        kept = jnp.exp(total)
        for h in range(n_heads):
            keys, vals = slice(h * key, (h + 1) * key), slice(h * val, (h + 1) * val)
            values = v_buf[at, vals]
            held = state[h]
            part[at, vals] = dot(scores[h].astype(jnp.bfloat16), values) + dot(
                entered[:, keys], held.astype(jnp.bfloat16), NT
            )
            state[h] = kept[:, keys] * held + dot(values, leaving[:, keys], TN)
        carry[...] = carry[...] + total

        @pl.when(i == spans // 2 - 1)
        def _():
            for d in range(1, n_groups):
                z_copy(d).wait_recv()
            for d in range(1, n_tp):
                tp_copy(d).start()

    def ends_copy(d):
        ref = ends.at[me]
        return pltpu.make_async_remote_copy(
            src_ref=ref, dst_ref=ref, send_sem=e_send.at[d - 1], recv_sem=e_recv.at[d - 1],
            device_id={"ep": lax.rem(me + d, n_ep)}, device_id_type=MESH,
        )

    high, low = high_low(carry[...])
    for h in range(n_heads):
        keys = slice(h * key, (h + 1) * key)
        ends[me, h, :val, :] = state[h].astype(jnp.bfloat16)
        ends[me, h, val:, :] = jnp.concatenate(
            [high[:, keys], low[:, keys], jnp.zeros((TAIL - 2, key), jnp.bfloat16)], axis=0
        )
    for d in range(1, n_ep):
        @pl.when(me + d < n_ep)
        def _(d=d):
            ends_copy(d).start()

    for d in range(1, n_tp):
        tp_copy(d).wait_recv()
    for d in range(1, members):
        member_copy(d).start()
    for d in range(1, n_ep):
        meta_copy(d).wait_recv()
    lane_group = lax.broadcasted_iota(jnp.int32, (8, lanes), 1) // room
    shift = (lane_group * SOURCE_STEP - mine_member * (experts * CAP)).astype(jnp.float32)
    chosen = []
    for m in range(members):
        found = shift
        for g in range(n_groups):
            found = found + meta_in[g * members + m]
        wanted = code_ref[:, m:m + 1]
        chosen.append(((wanted == found[0:1]) | (wanted == found[1:2])).astype(jnp.float32).astype(jnp.bfloat16))
    for d in range(1, members):
        member_copy(d).wait_recv()
    used = n_groups * room
    for s in range(n_tp):
        x = 0.0
        for m in range(members):
            x += dot(chosen[m][:, :used], rows_all[m, s].reshape(used, quarter))
        x = x.astype(jnp.bfloat16)
        for e in range(experts):
            x_buf[e, :, s * quarter:(s + 1) * quarter] = x[e * slots:(e + 1) * slots]

    def hidden_gather(e):
        return Gather(lambda owner, begin, size: hidden.at[e, owner, pl.ds(begin, size)], slots, n_tp, mt,
                      lambda k: h_send.at[e, k], lambda k: h_recv.at[e, k])

    @pl.loop(0, experts)
    def _(e):
        slot = lax.rem(e, slots_of_weights)
        for load in hidden_loads(e, slot):
            load.wait()
        x = x_buf[e]
        for j in range(ff // tile):
            at = slice(j * tile, (j + 1) * tile)
            gate = dot(x, gate_buf[slot, :, at])
            up = dot(x, up_buf[slot, :, at])
            hidden[e, mt, :, at] = (jax.nn.silu(gate) * up).astype(jnp.bfloat16)
        hidden_gather(e).start()

        @pl.when(e + slots_of_weights < experts)
        def _():
            for load in hidden_loads(e + slots_of_weights, slot):
                load.start()

    @pl.loop(0, experts)
    def _(e):
        hidden_gather(e).forward()

    for d in range(1, n_ep):
        @pl.when(me >= d)
        def _(d=d):
            ends_copy(d).wait_recv()
    for h in range(n_heads):
        def hop(place, held, h=h):
            kept = jnp.exp(ends[place, h, val:val + 1].astype(jnp.float32)
                           + ends[place, h, val + 1:val + 2].astype(jnp.float32))
            return kept * held + ends[place, h, :val].astype(jnp.float32)

        state[h] = lax.fori_loop(0, me, hop, jnp.zeros((val, key), jnp.float32))

    def heads_gather(i):
        return Gather(lambda owner, begin, size: heads_all.at[owner, pl.ds(aligned(i, span) + begin, size)], span, n_tp,
                      mt, lambda k: g_send.at[i, k], lambda k: g_recv.at[i, k])

    input_load(3).wait()

    @pl.loop(0, spans)
    def _(i):
        at = pl.ds(aligned(i, span), span)
        for h in range(n_heads):
            keys, vals = slice(h * key, (h + 1) * key), slice(h * val, (h + 1) * val)
            out = part[at, vals] + dot(decayed[at, keys], state[h].astype(jnp.bfloat16), NT)
            size = lax.rsqrt(jnp.mean(out * out, axis=-1, keepdims=True) + NORM_EPS)
            gated = out * size * gain_ref[...] * jax.nn.silu(og_buf[at, vals].astype(jnp.float32))
            heads_all[mt, at, vals] = gated.astype(jnp.bfloat16)
        heads_gather(i).start()

    @pl.loop(0, experts)
    def _(e):
        hidden_gather(e).finish()
        down_load(e).wait()
        total = 0.0
        for s in range(n_tp):
            total += dot(hidden[e, s], down_buf[e, s * ff:(s + 1) * ff])
        res[pl.ds(aligned(e, slots), slots), :] = total.astype(jnp.bfloat16)

    ordered = dot(order_ref[...], res[...]).astype(jnp.bfloat16)
    per_source = experts * CAP
    for s in range(n_ep):
        ret_out[s] = ordered[s * per_source:(s + 1) * per_source]

    def return_copy(d):
        to = lax.rem(me + d, n_ep)
        return pltpu.make_async_remote_copy(
            src_ref=ret_out.at[to], dst_ref=ret_in.at[me], send_sem=r_send.at[d - 1],
            recv_sem=r_recv.at[d - 1], device_id={"ep": to}, device_id_type=MESH,
        )

    for d in range(1, n_ep):
        return_copy(d).start()
    ret_in[me] = ret_out[me]

    @pl.loop(0, spans)
    def _(i):
        heads_gather(i).forward()

    input_load(4).wait()

    @pl.loop(0, spans)
    def _(i):
        heads_gather(i).finish()
        at = pl.ds(aligned(i, span), span)
        total = 0.0
        for s in range(n_tp):
            total += dot(heads_all[s, at], wout_buf[s * width:(s + 1) * width])
        mixed_ref[at, :] = total.astype(jnp.bfloat16)

    for d in range(1, n_ep):
        return_copy(d).wait_recv()
    spot = lax.broadcasted_iota(jnp.int32, (n_ep * per_source, row_count), 0)
    mix = jnp.where(spot == column[0], weight_ref[0:1, :], 0.0) + jnp.where(spot == column[1], weight_ref[1:2, :], 0.0)
    back = ret_in[...].reshape(n_ep * per_source, out_width)
    high, low = high_low(mix)
    expert_ref[...] = (dot(high, back, TN) + dot(low, back, TN)).astype(jnp.bfloat16)

    for d in range(1, n_groups):
        z_copy(d).wait_send()
    for d in range(1, n_tp):
        tp_copy(d).wait_send()
    for d in range(1, members):
        member_copy(d).wait_send()
    for d in range(1, n_ep):
        meta_copy(d).wait_send()
        return_copy(d).wait_send()

        @pl.when(me + d < n_ep)
        def _(d=d):
            ends_copy(d).wait_send()

    @pl.loop(0, experts)
    def _(e):
        hidden_gather(e).drain()

    @pl.loop(0, spans)
    def _(i):
        heads_gather(i).drain()


def local(
    recurrence_queries, forget_preact, recurrence_values, output_gate_preact, forget_floor_logits, surge_log_decay,
    head_norm_gain, recurrence_out_weight, second_micro_rows, expert_norm_gain, row_group_index, group_expert_index,
    chosen_expert_weight, expert_gate_weight, expert_up_weight, expert_down_weight,
):
    n_ep, n_tp = lax.axis_size("ep"), lax.axis_size("tp")
    length, width = recurrence_queries.shape
    vwidth = recurrence_values.shape[1]
    heads = surge_log_decay.shape[1]
    key, val = width // heads, vwidth // heads
    experts, model, ff = expert_gate_weight.shape
    out_width = expert_down_weight.shape[2]
    mix_width = recurrence_out_weight.shape[1]
    row_count = second_micro_rows.shape[0]
    members = n_ep // GROUPS
    per_group = experts * members
    room = min(row_count, per_group * CAP // 2)
    lanes = -(-GROUPS * room // 128) * 128
    slots = n_ep * CAP
    spans = length // SPAN
    quarter = model // n_tp
    stages = min(2, experts)
    steps = gather_steps(n_tp)
    bf, f32 = jnp.bfloat16, jnp.float32
    sums = jnp.asarray(log_sum_matrix(SPAN), bf)
    codes = jnp.asarray(slot_codes(n_ep, experts, members))
    order = jnp.asarray(by_source(n_ep, experts), bf)
    vmem, hbm = pl.BlockSpec(memory_space=pltpu.VMEM), pl.BlockSpec(memory_space=pl.ANY)
    buf, dma = pltpu.VMEM, pltpu.SemaphoreType.DMA
    weights = expert_gate_weight.size + expert_up_weight.size + expert_down_weight.size
    return pl.pallas_call(
        functools.partial(body, {"ep": n_ep, "tp": n_tp}),
        in_specs=[hbm] * 4 + [vmem] * 3 + [hbm] + [vmem] * 8 + [hbm] * 3,
        out_specs=[vmem, vmem],
        out_shape=[jax.ShapeDtypeStruct((length, mix_width), bf), jax.ShapeDtypeStruct((row_count, out_width), bf)],
        scratch_shapes=[
            buf((length, width), bf), buf((length, width), bf), buf((length, vwidth), bf), buf((length, vwidth), bf),
            buf(recurrence_out_weight.shape, bf),
            buf((length, vwidth), f32), buf((length, width), bf), buf((heads, val, key), f32), buf((1, width), f32),
            buf((n_ep, heads, val + TAIL, key), bf), buf((n_tp, length, vwidth), bf),
            buf((GROUPS, room, quarter), bf), buf((GROUPS, 8, lanes), f32), buf((n_ep, 8, lanes), f32),
            buf((members, n_tp, GROUPS, room, quarter), bf), buf((experts, slots, model), bf),
            buf((experts, n_tp, slots, ff), bf), buf((experts * slots, out_width), bf),
            buf((n_ep, experts * CAP, out_width), bf), buf((n_ep, experts * CAP, out_width), bf),
            buf((stages, model, ff), bf), buf((stages, model, ff), bf), buf(expert_down_weight.shape, bf),
            dma((5,)), dma((stages,)), dma((stages,)), dma((experts,)),
            dma((GROUPS - 1,)), dma((GROUPS - 1,)), dma((n_ep - 1,)), dma((n_ep - 1,)),
            dma((n_tp - 1,)), dma((n_tp - 1,)), dma((max(members - 1, 1),)), dma((max(members - 1, 1),)),
            dma((experts, steps)), dma((experts, steps)), dma((spans, steps)), dma((spans, steps)),
            dma((n_ep - 1,)), dma((n_ep - 1,)), dma((n_ep - 1,)), dma((n_ep - 1,)),
        ],
        compiler_params=pltpu.CompilerParams(collective_id=1, has_side_effects=True, vmem_limit_bytes=60 * 2**20),
        cost_estimate=pl.CostEstimate(flops=2 * slots * weights, bytes_accessed=2 * weights, transcendentals=0),
        name="layer",
    )(
        recurrence_queries, forget_preact, recurrence_values, output_gate_preact, forget_floor_logits[None, :],
        surge_log_decay.T, head_norm_gain[None, :], recurrence_out_weight, second_micro_rows, expert_norm_gain[None, :],
        row_group_index[None, :], group_expert_index.T, chosen_expert_weight.T, sums, codes, order,
        expert_gate_weight, expert_up_weight, expert_down_weight,
    )


def solution(mesh):
    return jax.shard_map(
        local,
        mesh=mesh,
        in_specs=(
            P("ep", "tp"),
            P("ep", "tp"),
            P("ep", "tp"),
            P("ep", "tp"),
            P("tp"),
            P("ep", "tp"),
            P(),
            P(None, "tp"),
            P("ep", None),
            P(),
            P("ep"),
            P("ep", None),
            P("ep", None),
            P("ep", None, "tp"),
            P("ep", None, "tp"),
            P("ep", None, "tp"),
        ),
        out_specs=(P("ep", "tp"), P("ep", "tp")),
        check_vma=False,
    )
```

time: 172 us -> 79 us (0.46)
  waiting for transfers between devices: 33.9 us -> 0 us
  blocking collectives: 18.6 us -> 0 us
  between operations: 14.2 us -> 0.65 us
  local copies, waits for them, and re-layouts: 15.9 us -> 3.44 us
  starting transfers between devices: 4.69 us -> 0 us
  other arithmetic: 4.47 us -> 0 us
  matrix products: 3.63 us -> 0 us
    all_gather x2 -> x0, waiting for transfers between devices: 21.4 us -> none  [the longest x1 21.4 us: token_mixing_layer(): ends = lax.all_gather(ending, 'ep')]
    all_to_all x1 -> x0, blocking collectives: 18.6 us -> none  [routed_experts(): lax.all_to_all(outgoing, 'ep', split_axis=0, concat_axis=1, tiled=True)]
    all_to_all x1 -> x0, waiting for transfers between devices: 12.4 us -> none  [routed_experts(): lax.all_to_all(result, 'ep', split_axis=1, concat_axis=0, tiled=True)]
    all_to_all x1 -> x0, starting transfers between devices: 4.61 us -> none  [routed_experts(): lax.all_to_all(result, 'ep', split_axis=1, concat_axis=0, tiled=True)]
    unnamed x14 -> x2, local copies, waits for them, and re-layouts: 7.61 us -> 3.44 us
    dot_general x1 -> x0, matrix products: 3.63 us -> none  [mixer_project(): jnp.dot(lax.all_gather(gated_heads, 'tp', axis=1, tiled=True), recurrence...]
    gather x2 -> x0, local copies, waits for them, and re-layouts: 3.22 us -> none  [the longest x1 2.06 us: routed_experts(): outgoing = padded[owner_row].reshape(expert_count, CAP, columns)]
    convert_element_type x3 -> x0, other arithmetic: 2.14 us -> none  [the longest x1 1.09 us: routed_experts(): rows_float = second_micro_rows.astype(jnp.float32)]
  transfers between devices with their start and end apart: 3 -> 0, of which waited for: 2 -> 0; matrix products, arithmetic and copies ran while one was open for 8% -> 0% of each run, Pallas kernels for 34% -> 0%
where the time goes in v1:
time: 79 us; the launch traced here: 78.8 us
  Pallas kernels  74.7 us (95%)
  local copies, waits for them, and re-layouts  3.44 us (4%)
    pallas_call x1, Pallas kernels, local(): pl.pallas_call(functools.partial(body, {'ep': n_ep, 'tp': n_tp}), in_spec...  74.7 us
    unnamed x2, local copies, waits for them, and re-layouts  3.44 us

profile of v1, /device:TPU:0, one launch (start us, length us, event | category | flops | bytes accessed | tf_op | source)
XLA Modules:
  0.0 78.8 jit_solution(10674851405377000837)
XLA Ops:
  0.6 74.7 %layer.1 = (bf16[512,512]{1,0:T(8,128)(2,1)}, bf16[128,512]{1,0:T(8,128)(2,1)}) custom-call(bf16[512,512]{1,0:T(8,128)(2,1)} %q_hbm.1, bf16[512,512]{1,0:T(8,128)(2,1)} %f_hbm.1, bf16[512,512]{1,0:T(8,128)(2,1)} %v_hbm.1, bf16[512,512]{1,0:T(8,128)(2,1)} %og_hbm.1, f32[1,512]{1,0:T(1,128)} %bitcast.9, f32[4,512]{1,0:T(4,128)} %bitcast.7, f32[1,128]{1,0:T(1,128)} %bitcast.12, ...), custom_call_target="tpu_custom_call" | custom-call | flops 4831838208 | bytes 50331648 | tf_op jit(solution)/shard_map/layer/pallas_call | solution.py:504
  75.3 1.9 %copy.23 = bf16[512,512]{1,0:T(8,128)(2,1)} copy(bf16[512,512]{1,0:T(8,128)(2,1)} %get-tuple-element.4) | data formatting | bytes 1048576
  77.2 1.6 %copy.24 = bf16[128,512]{1,0:T(8,128)(2,1)} copy(bf16[128,512]{1,0:T(8,128)(2,1)} %get-tuple-element.5) | data formatting | bytes 262144

commit v2 on v1

--- a/solution.py
+++ b/solution.py
@@ -62,6 +62,10 @@
     return pl.multiple_of(index * step, step)
 
 
+def wait_for(ref, semaphore):
+    pltpu.make_async_copy(ref, ref, semaphore).wait()
+
+
 class Gather:
     def __init__(self, pick, rows, count, me, send, recv):
         self.pick, self.rows, self.count, self.me, self.send, self.recv = pick, rows, count, me, send, recv
@@ -71,56 +75,39 @@
     def copy(self, k, owner, begin, size, peer):
         ref = self.pick(owner, begin, size)
         return pltpu.make_async_remote_copy(
-            src_ref=ref, dst_ref=ref, send_sem=self.send(k), recv_sem=self.recv(k),
+            src_ref=ref, dst_ref=ref, send_sem=self.send, recv_sem=self.recv(k),
             device_id={"tp": peer}, device_id_type=MESH,
         )
 
-    def first(self):
-        if not self.square:
-            return [self.copy(d - 1, self.me, 0, self.rows, lax.rem(self.me + d, self.count))
-                    for d in range(1, self.count)]
-        return [self.copy(k, self.me, 0, self.rows, self.me ^ (1 << k)) for k in range(2)]
-
-    def second(self):
-        if not self.square:
-            return []
-        return [self.copy(2, self.me ^ 1, 0, self.half, self.me ^ 2),
-                self.copy(3, self.me ^ 2, self.half, self.half, self.me ^ 1)]
-
     def start(self):
-        for copy in self.first():
-            copy.start()
+        peers = [self.me ^ 1, self.me ^ 2] if self.square else [
+            lax.rem(self.me + d, self.count) for d in range(1, self.count)]
+        for peer in peers:
+            self.copy(0, self.me, 0, self.rows, peer).start()
 
     def forward(self):
         if self.square:
-            for came, passed in zip(self.first(), self.second()):
-                came.wait_recv()
-                passed.start()
+            wait_for(self.pick(pl.ds(0, 2), 0, self.rows), self.recv(0))
+            self.copy(1, self.me ^ 1, 0, self.half, self.me ^ 2).start()
+            self.copy(1, self.me ^ 2, self.half, self.half, self.me ^ 1).start()
 
     def finish(self):
-        for copy in self.second() if self.square else self.first():
-            copy.wait_recv()
-
-    def drain(self):
-        for copy in self.first() + self.second():
-            copy.wait_send()
-
-
-def gather_steps(count):
-    return 4 if count == 4 else count - 1
-
-
-def body(
-    dims,
-    q_hbm, f_hbm, v_hbm, og_hbm, floor_ref, surge_ref, gain_ref, wout_hbm, rows_ref, egain_ref, grp_ref, pick_ref,
-    weight_ref, sums_ref, code_ref, order_ref, gate_hbm, up_hbm, down_hbm,
-    mixed_ref, expert_ref,
-    q_buf, f_buf, v_buf, og_buf, wout_buf, part, decayed, state, carry, ends, heads_all,
-    pack, meta_out, meta_in, rows_all, x_buf, hidden, res, ret_out, ret_in, gate_buf, up_buf, down_buf,
-    in_sem, gate_sem, up_sem, down_sem,
-    z_send, z_recv, m_send, m_recv, t_send, t_recv, d_send, d_recv,
-    h_send, h_recv, g_send, g_recv, e_send, e_recv, r_send, r_recv,
-):
+        blocks = 1 if self.square else self.count - 1
+        wait_for(self.pick(pl.ds(0, blocks), 0, self.rows), self.recv(1 if self.square else 0))
+
+
+LOADED = 16
+
+
+def body(dims, *refs):
+    sources, refs = refs[:LOADED], refs[LOADED:]
+    (gate_hbm, up_hbm, down_hbm, mixed_ref, expert_ref), refs = refs[:5], refs[5:]
+    loaded, refs = refs[:LOADED], refs[LOADED:]
+    (floor_ref, surge_ref, gain_ref, rows_ref, egain_ref, grp_ref, pick_ref, weight_ref, sums_ref, code_ref, order_ref,
+     q_buf, f_buf, v_buf, og_buf, wout_buf) = loaded
+    (part, decayed, state, carry, ends, heads_all, pack, meta_out, meta_in, rows_all, x_buf, hidden, res, ret_out, ret_in,
+     gate_buf, up_buf, down_buf, in_sem, gate_sem, up_sem, down_sem, z_send, z_recv, m_send, m_recv, t_send, t_recv,
+     d_send, d_recv, h_send, h_recv, g_send, g_recv, e_send, e_recv, f_send, f_recv, r_send, r_recv) = refs
     n_ep, n_tp, n_groups = dims["ep"], dims["tp"], GROUPS
     members = n_ep // n_groups
     me, mt = lax.axis_index("ep"), lax.axis_index("tp")
@@ -135,6 +122,7 @@
     row_count, model = rows_ref.shape
     quarter = model // n_tp
     room = pack.shape[1]
+    halves = hidden.shape[0] // gate_hbm.shape[0]
     lanes = meta_out.shape[2]
     slots = x_buf.shape[1]
     ff = hidden.shape[3]
@@ -142,8 +130,7 @@
     out_width = mixed_ref.shape[1]
 
     def input_load(k):
-        pair = [(q_hbm, q_buf), (f_hbm, f_buf), (v_hbm, v_buf), (og_hbm, og_buf), (wout_hbm, wout_buf)][k]
-        return pltpu.make_async_copy(pair[0], pair[1], in_sem.at[k])
+        return pltpu.make_async_copy(sources[k], loaded[k], in_sem.at[k])
 
     def hidden_loads(e, slot):
         return (pltpu.make_async_copy(gate_hbm.at[e], gate_buf.at[slot], gate_sem.at[slot]),
@@ -157,7 +144,7 @@
         pl.semaphore_signal(barrier, inc=1, device_id={"tp": lax.rem(mt + d, n_tp)}, device_id_type=MESH)
     for d in range(1, n_ep):
         pl.semaphore_signal(barrier, inc=1, device_id={"ep": lax.rem(me + d, n_ep)}, device_id_type=MESH)
-    for k in range(4):
+    for k in (3, 4, 5, 6, 11, 12, 13, 0, 1, 8, 2, 7, 9, 10, 14):
         input_load(k).start()
     slots_of_weights = gate_buf.shape[0]
     for e in range(min(slots_of_weights, experts)):
@@ -165,8 +152,10 @@
             load.start()
     for e in range(experts):
         down_load(e).start()
-    input_load(4).start()
-
+    input_load(15).start()
+
+    for k in (5, 6):
+        input_load(k).wait()
     grp = grp_ref[...]
     picks = [pick_ref[c:c + 1, :] for c in range(2)]
     n_experts = per_group * n_groups
@@ -193,6 +182,8 @@
         at = ((spot == mine_group * room + place) & (grp == g)).astype(jnp.float32).astype(jnp.bfloat16)
         meta_out[g] = dot(codes, at, NT)
 
+    for k in (3, 4):
+        input_load(k).wait()
     rows_float = rows_ref[...].astype(jnp.float32)
     scale = lax.rsqrt(jnp.mean(rows_float * rows_float, axis=-1, keepdims=True) + NORM_EPS)
     columns = pl.ds(aligned(mt, quarter), quarter)
@@ -202,49 +193,63 @@
     packed = dot(at, normed).astype(jnp.bfloat16)
     for g in range(n_groups):
         pack[g] = packed[g * room:(g + 1) * room]
-
-    def z_copy(d):
-        g = lax.rem(mine_group + d, n_groups)
+    rows_all[mine_member, mine_group, mt] = pack[mine_group]
+    meta_in[me] = meta_out[mine_group]
+
+    def z_copy(p):
+        g = mine_group ^ p
         return pltpu.make_async_remote_copy(
-            src_ref=pack.at[g], dst_ref=rows_all.at[mine_member, mt, mine_group], send_sem=z_send.at[d - 1],
-            recv_sem=z_recv.at[d - 1], device_id={"ep": g * members + mine_member}, device_id_type=MESH,
+            src_ref=pack.at[g], dst_ref=rows_all.at[mine_member, mine_group, mt], send_sem=z_send.at[0],
+            recv_sem=z_recv.at[p - 1], device_id={"ep": g * members + mine_member}, device_id_type=MESH,
         )
 
     def meta_copy(d):
         to = lax.rem(me + d, n_ep)
         return pltpu.make_async_remote_copy(
-            src_ref=meta_out.at[to // members], dst_ref=meta_in.at[me], send_sem=m_send.at[d - 1],
-            recv_sem=m_recv.at[d - 1], device_id={"ep": to}, device_id_type=MESH,
-        )
-
-    def tp_copy(d):
-        ref = rows_all.at[mine_member, mt]
-        return pltpu.make_async_remote_copy(
-            src_ref=ref, dst_ref=ref, send_sem=t_send.at[d - 1], recv_sem=t_recv.at[d - 1],
+            src_ref=meta_out.at[to // members], dst_ref=meta_in.at[me], send_sem=m_send.at[0],
+            recv_sem=m_recv.at[0], device_id={"ep": to}, device_id_type=MESH,
+        )
+
+    def tp_copies(p):
+        ref = rows_all.at[mine_member, mine_group ^ p, mt]
+        return [pltpu.make_async_remote_copy(
+            src_ref=ref, dst_ref=ref, send_sem=t_send.at[0], recv_sem=t_recv.at[p],
             device_id={"tp": lax.rem(mt + d, n_tp)}, device_id_type=MESH,
-        )
-
-    def member_copy(d):
-        to = mine_group * members + lax.rem(mine_member + d, members)
-        ref = rows_all.at[mine_member]
-        return pltpu.make_async_remote_copy(
-            src_ref=ref, dst_ref=ref, send_sem=d_send.at[d - 1], recv_sem=d_recv.at[d - 1],
-            device_id={"ep": to}, device_id_type=MESH,
-        )
+        ) for d in range(1, n_tp)]
+
+    def member_copies(p):
+        ref = rows_all.at[mine_member, mine_group ^ p]
+        return [pltpu.make_async_remote_copy(
+            src_ref=ref, dst_ref=ref, send_sem=d_send.at[0], recv_sem=d_recv.at[0],
+            device_id={"ep": mine_group * members + lax.rem(mine_member + d, members)}, device_id_type=MESH,
+        ) for d in range(1, members)]
+
+    def to_members(p):
+        wait_for(rows_all.at[0, 0, pl.ds(0, n_tp - 1)], t_recv.at[p])
+        for copy in member_copies(p):
+            copy.start()
+
+    def dispatch(stage):
+        if stage + 1 < n_groups:
+            z_copy(stage + 1).wait_recv()
+            for copy in tp_copies(stage + 1):
+                copy.start()
+        if stage > 0:
+            to_members(stage - 1)
 
     pl.semaphore_wait(barrier, n_tp + n_ep - 2)
-    for d in range(1, n_groups):
-        z_copy(d).start()
+    for p in range(1, n_groups):
+        z_copy(p).start()
+    for copy in tp_copies(0):
+        copy.start()
     for d in range(1, n_ep):
         meta_copy(d).start()
-    rows_all[mine_member, mt, mine_group] = pack[mine_group]
-    meta_in[me] = meta_out[mine_group]
 
     state[...] = jnp.zeros_like(state)
     carry[...] = jnp.zeros_like(carry)
+    for k in (0, 1, 8, 11, 12, 13):
+        input_load(k).wait()
     rate = jax.nn.sigmoid(-floor_ref[...])
-    for k in range(3):
-        input_load(k).wait()
 
     @pl.loop(0, spans)
     def _(i):
@@ -293,19 +298,24 @@
             state[h] = kept[:, keys] * held + dot(values, leaving[:, keys], TN)
         carry[...] = carry[...] + total
 
-        @pl.when(i == spans // 2 - 1)
-        def _():
-            for d in range(1, n_groups):
-                z_copy(d).wait_recv()
-            for d in range(1, n_tp):
-                tp_copy(d).start()
-
-    def ends_copy(d):
+        for stage in range(n_groups):
+            @pl.when(i == min(stage, spans - 1))
+            def _(stage=stage):
+                dispatch(stage)
+
+    def ends_copy(p):
         ref = ends.at[me]
         return pltpu.make_async_remote_copy(
-            src_ref=ref, dst_ref=ref, send_sem=e_send.at[d - 1], recv_sem=e_recv.at[d - 1],
-            device_id={"ep": lax.rem(me + d, n_ep)}, device_id_type=MESH,
-        )
+            src_ref=ref, dst_ref=ref, send_sem=e_send.at[p - 1], recv_sem=e_recv.at[p - 1],
+            device_id={"ep": lax.rem(me + p * members, n_ep)}, device_id_type=MESH,
+        )
+
+    def ends_passed(p):
+        ref = ends.at[lax.rem(me - p * members + n_ep, n_ep)]
+        return [pltpu.make_async_remote_copy(
+            src_ref=ref, dst_ref=ref, send_sem=f_send.at[p, d - 1], recv_sem=f_recv.at[p, d - 1],
+            device_id={"ep": mine_group * members + lax.rem(mine_member + d, members)}, device_id_type=MESH,
+        ) for d in range(1, members)]
 
     high, low = high_low(carry[...])
     for h in range(n_heads):
@@ -314,17 +324,17 @@
         ends[me, h, val:, :] = jnp.concatenate(
             [high[:, keys], low[:, keys], jnp.zeros((TAIL - 2, key), jnp.bfloat16)], axis=0
         )
-    for d in range(1, n_ep):
-        @pl.when(me + d < n_ep)
-        def _(d=d):
-            ends_copy(d).start()
-
-    for d in range(1, n_tp):
-        tp_copy(d).wait_recv()
-    for d in range(1, members):
-        member_copy(d).start()
-    for d in range(1, n_ep):
-        meta_copy(d).wait_recv()
+    for p in range(1, n_groups):
+        @pl.when(mine_group + p < n_groups)
+        def _(p=p):
+            ends_copy(p).start()
+
+    for copy in ends_passed(0):
+        copy.start()
+
+    to_members(n_groups - 1)
+    wait_for(meta_in.at[pl.ds(0, n_ep - 1)], m_recv.at[0])
+    input_load(9).wait()
     lane_group = lax.broadcasted_iota(jnp.int32, (8, lanes), 1) // room
     shift = (lane_group * SOURCE_STEP - mine_member * (experts * CAP)).astype(jnp.float32)
     chosen = []
@@ -334,20 +344,19 @@
             found = found + meta_in[g * members + m]
         wanted = code_ref[:, m:m + 1]
         chosen.append(((wanted == found[0:1]) | (wanted == found[1:2])).astype(jnp.float32).astype(jnp.bfloat16))
-    for d in range(1, members):
-        member_copy(d).wait_recv()
+    wait_for(rows_all.at[pl.ds(0, members - 1)], d_recv.at[0])
     used = n_groups * room
     for s in range(n_tp):
         x = 0.0
         for m in range(members):
-            x += dot(chosen[m][:, :used], rows_all[m, s].reshape(used, quarter))
+            x += dot(chosen[m][:, :used], rows_all[m, :, s].reshape(used, quarter))
         x = x.astype(jnp.bfloat16)
         for e in range(experts):
             x_buf[e, :, s * quarter:(s + 1) * quarter] = x[e * slots:(e + 1) * slots]
 
-    def hidden_gather(e):
-        return Gather(lambda owner, begin, size: hidden.at[e, owner, pl.ds(begin, size)], slots, n_tp, mt,
-                      lambda k: h_send.at[e, k], lambda k: h_recv.at[e, k])
+    def hidden_gather(c):
+        return Gather(lambda owner, begin, size: hidden.at[c, owner, pl.ds(begin, size)], slots, n_tp, mt,
+                      h_send.at[0], lambda k: h_recv.at[c, k])
 
     @pl.loop(0, experts)
     def _(e):
@@ -355,26 +364,38 @@
         for load in hidden_loads(e, slot):
             load.wait()
         x = x_buf[e]
-        for j in range(ff // tile):
-            at = slice(j * tile, (j + 1) * tile)
-            gate = dot(x, gate_buf[slot, :, at])
-            up = dot(x, up_buf[slot, :, at])
-            hidden[e, mt, :, at] = (jax.nn.silu(gate) * up).astype(jnp.bfloat16)
-        hidden_gather(e).start()
+        for part_at in range(halves):
+            for j in range(ff // tile):
+                at = slice(j * tile, (j + 1) * tile)
+                from_at = slice(part_at * ff + j * tile, part_at * ff + (j + 1) * tile)
+                gate = dot(x, gate_buf[slot, :, from_at])
+                up = dot(x, up_buf[slot, :, from_at])
+                hidden[e * halves + part_at, mt, :, at] = (jax.nn.silu(gate) * up).astype(jnp.bfloat16)
+            hidden_gather(e * halves + part_at).start()
 
         @pl.when(e + slots_of_weights < experts)
         def _():
             for load in hidden_loads(e + slots_of_weights, slot):
                 load.start()
 
-    @pl.loop(0, experts)
-    def _(e):
-        hidden_gather(e).forward()
-
-    for d in range(1, n_ep):
-        @pl.when(me >= d)
-        def _(d=d):
-            ends_copy(d).wait_recv()
+    @pl.loop(0, experts * halves)
+    def _(c):
+        hidden_gather(c).forward()
+
+        @pl.when(c == experts * halves // 2)
+        def _():
+            for p in range(1, n_groups):
+                @pl.when(mine_group >= p)
+                def _(p=p):
+                    ends_copy(p).wait_recv()
+                    for copy in ends_passed(p):
+                        copy.start()
+
+    for p in range(n_groups):
+        @pl.when(mine_group >= p)
+        def _(p=p):
+            for copy in ends_passed(p):
+                copy.wait_recv()
     for h in range(n_heads):
         def hop(place, held, h=h):
             kept = jnp.exp(ends[place, h, val:val + 1].astype(jnp.float32)
@@ -385,9 +406,10 @@
 
     def heads_gather(i):
         return Gather(lambda owner, begin, size: heads_all.at[owner, pl.ds(aligned(i, span) + begin, size)], span, n_tp,
-                      mt, lambda k: g_send.at[i, k], lambda k: g_recv.at[i, k])
-
-    input_load(3).wait()
+                      mt, g_send.at[0], lambda k: g_recv.at[i, k])
+
+    for k in (2, 14):
+        input_load(k).wait()
 
     @pl.loop(0, spans)
     def _(i):
@@ -402,13 +424,16 @@
 
     @pl.loop(0, experts)
     def _(e):
-        hidden_gather(e).finish()
         down_load(e).wait()
         total = 0.0
-        for s in range(n_tp):
-            total += dot(hidden[e, s], down_buf[e, s * ff:(s + 1) * ff])
+        for part_at in range(halves):
+            hidden_gather(e * halves + part_at).finish()
+            for s in range(n_tp):
+                begin = (s * halves + part_at) * ff
+                total += dot(hidden[e * halves + part_at, s], down_buf[e, begin:begin + ff])
         res[pl.ds(aligned(e, slots), slots), :] = total.astype(jnp.bfloat16)
 
+    input_load(10).wait()
     ordered = dot(order_ref[...], res[...]).astype(jnp.bfloat16)
     per_source = experts * CAP
     for s in range(n_ep):
@@ -417,8 +442,8 @@
     def return_copy(d):
         to = lax.rem(me + d, n_ep)
         return pltpu.make_async_remote_copy(
-            src_ref=ret_out.at[to], dst_ref=ret_in.at[me], send_sem=r_send.at[d - 1],
-            recv_sem=r_recv.at[d - 1], device_id={"ep": to}, device_id_type=MESH,
+            src_ref=ret_out.at[to], dst_ref=ret_in.at[me], send_sem=r_send.at[0],
+            recv_sem=r_recv.at[0], device_id={"ep": to}, device_id_type=MESH,
         )
 
     for d in range(1, n_ep):
@@ -429,7 +454,32 @@
     def _(i):
         heads_gather(i).forward()
 
-    input_load(4).wait()
+    input_load(7).wait()
+    wait_for(ret_in.at[pl.ds(0, n_ep - 1)], r_recv.at[0])
+    spot = lax.broadcasted_iota(jnp.int32, (n_ep * per_source, row_count), 0)
+    mix = jnp.where(spot == column[0], weight_ref[0:1, :], 0.0) + jnp.where(spot == column[1], weight_ref[1:2, :], 0.0)
+    back = ret_in[...].reshape(n_ep * per_source, out_width)
+    high, low = high_low(mix)
+    expert_ref[...] = (dot(high, back, TN) + dot(low, back, TN)).astype(jnp.bfloat16)
+
+    wait_for(pack.at[pl.ds(0, n_groups - 1)], z_send.at[0])
+    wait_for(rows_all.at[0, :, pl.ds(0, n_tp - 1)], t_send.at[0])
+    wait_for(rows_all.at[pl.ds(0, members - 1)], d_send.at[0])
+    wait_for(meta_in.at[pl.ds(0, n_ep - 1)], m_send.at[0])
+    wait_for(ret_in.at[pl.ds(0, n_ep - 1)], r_send.at[0])
+    wait_for(hidden.at[:, pl.ds(0, n_tp - 1)], h_send.at[0])
+    for p in range(n_groups):
+        if p:
+            @pl.when(mine_group + p < n_groups)
+            def _(p=p):
+                ends_copy(p).wait_send()
+
+        @pl.when(mine_group >= p)
+        def _(p=p):
+            for copy in ends_passed(p):
+                copy.wait_send()
+
+    input_load(15).wait()
 
     @pl.loop(0, spans)
     def _(i):
@@ -440,35 +490,7 @@
             total += dot(heads_all[s, at], wout_buf[s * width:(s + 1) * width])
         mixed_ref[at, :] = total.astype(jnp.bfloat16)
 
-    for d in range(1, n_ep):
-        return_copy(d).wait_recv()
-    spot = lax.broadcasted_iota(jnp.int32, (n_ep * per_source, row_count), 0)
-    mix = jnp.where(spot == column[0], weight_ref[0:1, :], 0.0) + jnp.where(spot == column[1], weight_ref[1:2, :], 0.0)
-    back = ret_in[...].reshape(n_ep * per_source, out_width)
-    high, low = high_low(mix)
-    expert_ref[...] = (dot(high, back, TN) + dot(low, back, TN)).astype(jnp.bfloat16)
-
-    for d in range(1, n_groups):
-        z_copy(d).wait_send()
-    for d in range(1, n_tp):
-        tp_copy(d).wait_send()
-    for d in range(1, members):
-        member_copy(d).wait_send()
-    for d in range(1, n_ep):
-        meta_copy(d).wait_send()
-        return_copy(d).wait_send()
-
-        @pl.when(me + d < n_ep)
-        def _(d=d):
-            ends_copy(d).wait_send()
-
-    @pl.loop(0, experts)
-    def _(e):
-        hidden_gather(e).drain()
-
-    @pl.loop(0, spans)
-    def _(i):
-        heads_gather(i).drain()
+    wait_for(heads_all.at[pl.ds(0, n_tp - 1)], g_send.at[0])
 
 
 def local(
@@ -493,44 +515,44 @@
     spans = length // SPAN
     quarter = model // n_tp
     stages = min(2, experts)
-    steps = gather_steps(n_tp)
+    steps = 2 if n_tp == 4 else 1
     bf, f32 = jnp.bfloat16, jnp.float32
     sums = jnp.asarray(log_sum_matrix(SPAN), bf)
     codes = jnp.asarray(slot_codes(n_ep, experts, members))
     order = jnp.asarray(by_source(n_ep, experts), bf)
-    vmem, hbm = pl.BlockSpec(memory_space=pltpu.VMEM), pl.BlockSpec(memory_space=pl.ANY)
+    vmem, hbm = pl.BlockSpec(memory_space=pltpu.VMEM), pl.BlockSpec(memory_space=pltpu.HBM)
     buf, dma = pltpu.VMEM, pltpu.SemaphoreType.DMA
     weights = expert_gate_weight.size + expert_up_weight.size + expert_down_weight.size
+    loaded = [
+        forget_floor_logits[None, :], surge_log_decay.T, head_norm_gain[None, :], second_micro_rows,
+        expert_norm_gain[None, :], row_group_index[None, :], group_expert_index.T, chosen_expert_weight.T, sums, codes,
+        order, recurrence_queries, forget_preact, recurrence_values, output_gate_preact, recurrence_out_weight,
+    ]
+    halves = 2 if ff % 512 == 0 else 1
+    chunks = experts * halves
     return pl.pallas_call(
         functools.partial(body, {"ep": n_ep, "tp": n_tp}),
-        in_specs=[hbm] * 4 + [vmem] * 3 + [hbm] + [vmem] * 8 + [hbm] * 3,
+        in_specs=[hbm] * (LOADED + 3),
         out_specs=[vmem, vmem],
         out_shape=[jax.ShapeDtypeStruct((length, mix_width), bf), jax.ShapeDtypeStruct((row_count, out_width), bf)],
-        scratch_shapes=[
-            buf((length, width), bf), buf((length, width), bf), buf((length, vwidth), bf), buf((length, vwidth), bf),
-            buf(recurrence_out_weight.shape, bf),
+        scratch_shapes=[buf(array.shape, array.dtype) for array in loaded] + [
             buf((length, vwidth), f32), buf((length, width), bf), buf((heads, val, key), f32), buf((1, width), f32),
             buf((n_ep, heads, val + TAIL, key), bf), buf((n_tp, length, vwidth), bf),
             buf((GROUPS, room, quarter), bf), buf((GROUPS, 8, lanes), f32), buf((n_ep, 8, lanes), f32),
-            buf((members, n_tp, GROUPS, room, quarter), bf), buf((experts, slots, model), bf),
-            buf((experts, n_tp, slots, ff), bf), buf((experts * slots, out_width), bf),
+            buf((members, GROUPS, n_tp, room, quarter), bf), buf((experts, slots, model), bf),
+            buf((chunks, n_tp, slots, ff // halves), bf), buf((experts * slots, out_width), bf),
             buf((n_ep, experts * CAP, out_width), bf), buf((n_ep, experts * CAP, out_width), bf),
             buf((stages, model, ff), bf), buf((stages, model, ff), bf), buf(expert_down_weight.shape, bf),
-            dma((5,)), dma((stages,)), dma((stages,)), dma((experts,)),
-            dma((GROUPS - 1,)), dma((GROUPS - 1,)), dma((n_ep - 1,)), dma((n_ep - 1,)),
-            dma((n_tp - 1,)), dma((n_tp - 1,)), dma((max(members - 1, 1),)), dma((max(members - 1, 1),)),
-            dma((experts, steps)), dma((experts, steps)), dma((spans, steps)), dma((spans, steps)),
-            dma((n_ep - 1,)), dma((n_ep - 1,)), dma((n_ep - 1,)), dma((n_ep - 1,)),
+            dma((LOADED,)), dma((stages,)), dma((stages,)), dma((experts,)),
+            dma((1,)), dma((GROUPS - 1,)), dma((1,)), dma((1,)), dma((1,)), dma((GROUPS,)), dma((1,)), dma((1,)),
+            dma((1,)), dma((chunks, steps)), dma((1,)), dma((spans, steps)),
+            dma((GROUPS - 1,)), dma((GROUPS - 1,)), dma((GROUPS, members - 1)), dma((GROUPS, members - 1)),
+            dma((1,)), dma((1,)),
         ],
-        compiler_params=pltpu.CompilerParams(collective_id=1, has_side_effects=True, vmem_limit_bytes=60 * 2**20),
+        compiler_params=pltpu.CompilerParams(collective_id=1, has_side_effects=True, vmem_limit_bytes=52 * 2**20),
         cost_estimate=pl.CostEstimate(flops=2 * slots * weights, bytes_accessed=2 * weights, transcendentals=0),
         name="layer",
-    )(
-        recurrence_queries, forget_preact, recurrence_values, output_gate_preact, forget_floor_logits[None, :],
-        surge_log_decay.T, head_norm_gain[None, :], recurrence_out_weight, second_micro_rows, expert_norm_gain[None, :],
-        row_group_index[None, :], group_expert_index.T, chosen_expert_weight.T, sums, codes, order,
-        expert_gate_weight, expert_up_weight, expert_down_weight,
-    )
+    )(*[pltpu.with_memory_space_constraint(array, pltpu.HBM) for array in loaded], expert_gate_weight, expert_up_weight, expert_down_weight)
 
 
 def solution(mesh):

time: 79 us -> 68.6 us (0.87)
  Pallas kernels: 74.7 us -> 66.4 us
  local copies, waits for them, and re-layouts: 3.44 us -> 1.45 us
    pallas_call x1, Pallas kernels: 74.7 us -> 66.4 us  [local(): pl.pallas_call(functools.partial(body, {'ep': n_ep, 'tp': n_tp}), in_spec...]
    unnamed x2, local copies, waits for them, and re-layouts: 3.44 us -> 1.45 us
where the time goes in v2:
time: 68.6 us; the launch traced here: 68.5 us
  Pallas kernels  66.4 us (97%)
  local copies, waits for them, and re-layouts  1.45 us (2%)
    pallas_call x1, Pallas kernels, local(): pl.pallas_call(functools.partial(body, {'ep': n_ep, 'tp': n_tp}), in_spec...  66.4 us
    unnamed x2, local copies, waits for them, and re-layouts  1.45 us

profile of v2, /device:TPU:0, one launch (start us, length us, event | category | flops | bytes accessed | tf_op | source)
XLA Modules:
  0.0 68.5 jit_solution(7012363526074236795)
XLA Ops:
  0.6 66.4 %layer.1 = (bf16[512,512]{1,0:T(8,128)(2,1)S(1)}, bf16[128,512]{1,0:T(8,128)(2,1)S(1)}) custom-call(f32[1,512]{1,0:T(1,128)} %bitcast.9, f32[4,512]{1,0:T(4,128)} %bitcast.7, f32[1,128]{1,0:T(1,128)} %bitcast.12, bf16[128,2048]{1,0:T(8,128)(2,1)} %refs_3_.1, f32[1,2048]{1,0:T(1,128)} %bitcast.8, s32[1,128]{1,0:T(1,128)} %bitcast.13, s32[2,128]{1,0:T(2,128)} %bitcast.10, ...), custom_call_target="tpu_custom_call" | custom-call | flops 4831838208 | bytes 50331648 | tf_op jit(solution)/shard_map/layer/pallas_call | solution.py:533
  67.0 0.8 %copy.23 = bf16[512,512]{1,0:T(8,128)(2,1)} copy(bf16[512,512]{1,0:T(8,128)(2,1)S(1)} %get-tuple-element.4) | data formatting | bytes 1048576
  67.8 0.7 copy.24
